TPU v7x, 32 devices: a whole 2x2x4 slice. The times are simulated.
32 devices in a mesh: dp: 4 (over y, x), kv: 4 (over z), tp: 2 (over core).
Axes of the slice: x: 2, y: 2, z: 4, core: 2. Of those that a mesh axis runs over, the one named last changes fastest.
Arguments:
- tokens: bfloat16 [8192, 2048], P(('dp', 'kv')), parts along dimension 0, may hold values from -60 to 60, as said below
- chosen: int32 [128, 16], P(('dp', 'kv')), parts along dimension 0, may hold values from -1 to 31, as said below
- query_weight: bfloat16 [2048, 1024], P('kv', 'tp'), may hold values from -0.125 to 0.125
- key_matrix: bfloat16 [2048, 128], P('kv', 'tp'), may hold values from -0.125 to 0.125
- value_matrix: bfloat16 [2048, 128], P('kv', 'tp'), may hold values from -0.125 to 0.125
- out_weight: bfloat16 [1024, 2048], P('tp', 'kv'), may hold values from -0.1875 to 0.1875
- out_gain: float32 [2048], replicated, may hold values from 0.1 to 1.9
Outputs:
- mixed_out: bfloat16 [8192, 2048], P(('dp', 'kv', 'tp')), parts along dimension 0
There are 4 independent parts, one for each index of `dp`. A program takes and returns all parts, laid end to end along the dimension named above; an argument that names none is the same for every part. Nothing has to cross between parts.
Inputs may be any that keep to these rules, and one draw needn't show every extreme that they name: tokens are of order one apart from few rows. chosen[g, 0] = g; every other entry of row g is -1 or a block below g, and the entries of a row other than -1 are distinct; the blocks that the rows of one device name on any single other device are at most 2 different ones, and this is reached.
All inputs are finite; a program needn't handle non-finite values.
Results may differ from a plain program's by a relative error of at most 0.012.
The roundings to bfloat16 on the way count: a program that leaves them out, or rounds other values in their place, can miss the bound.
Values may be sent and summed in bfloat16 or wider, within the bound.
A program may use at most 64 MiB of HBM per device.

v0:
```python
import jax
import jax.numpy as jnp
from jax import lax
from jax.sharding import PartitionSpec as P

HEAD_WIDTH = 64
BLOCK_LENGTH = 64


def per_device(tokens, chosen, query_weight, key_matrix, value_matrix, out_weight, out_gain):
    tok_rows = tokens.shape[0]
    blocks = tok_rows // BLOCK_LENGTH
    device = lax.axis_index("kv")
    kv_count = lax.axis_size("kv")
    whole_query, whole_key, whole_value = (
        lax.all_gather(query_weight, "kv", axis=0, tiled=True),
        lax.all_gather(key_matrix, "kv", axis=0, tiled=True),
        lax.all_gather(value_matrix, "kv", axis=0, tiled=True),
    )
    query_rows = jnp.dot(tokens, whole_query, preferred_element_type=jnp.float32).astype(
        jnp.bfloat16
    )
    key_rows = jnp.dot(tokens, whole_key, preferred_element_type=jnp.float32).astype(jnp.bfloat16)
    value_rows = jnp.dot(tokens, whole_value, preferred_element_type=jnp.float32).astype(
        jnp.bfloat16
    )
    paired = jnp.concatenate([key_rows, value_rows], axis=1)
    pair_width = paired.shape[1]
    safe_ids = jnp.maximum(chosen, 0)
    everyone = lax.all_gather(paired, "kv", axis=0, tiled=True).reshape(
        kv_count * blocks, BLOCK_LENGTH, pair_width
    )
    picked = jnp.take(everyone, safe_ids, axis=0)
    head_count = query_rows.shape[1] // HEAD_WIDTH
    grouped = query_rows.reshape(blocks, BLOCK_LENGTH, head_count, HEAD_WIDTH)
    offsets = jnp.arange(BLOCK_LENGTH, dtype=jnp.int32)
    query_pos = (device * blocks + jnp.arange(blocks, dtype=jnp.int32))[
        :, None
    ] * BLOCK_LENGTH + offsets[None, :]
    key_pos = safe_ids[:, :, None] * BLOCK_LENGTH + offsets[None, None, :]
    visible = (chosen >= 0)[:, None, :, None] & (
        key_pos[:, None, :, :] <= query_pos[:, :, None, None]
    )

    def attend_block(inputs):
        query_block, pair_block, seen = inputs
        block_keys = pair_block[..., :HEAD_WIDTH]
        block_values = pair_block[..., HEAD_WIDTH:]
        scores = jnp.einsum(
            "qgd,skd->gqsk", query_block, block_keys, preferred_element_type=jnp.float32
        ) * HEAD_WIDTH ** (-0.5)
        scores = jnp.where(seen[None], scores, -1e30)
        row_max = jnp.max(scores, axis=(2, 3), keepdims=True)
        expon = jnp.exp(scores - row_max)
        row_sum = jnp.sum(expon, axis=(2, 3), keepdims=True)
        weights_bf = (expon / row_sum).astype(jnp.bfloat16)
        result = jnp.einsum(
            "gqsk,skd->qgd", weights_bf, block_values, preferred_element_type=jnp.float32
        )
        return result.astype(jnp.bfloat16)

    attended = lax.map(attend_block, (grouped, picked, visible))
    attended = attended.reshape(tok_rows, head_count * HEAD_WIDTH)
    whole_out = lax.all_gather(out_weight, "kv", axis=1, tiled=True)
    mixed = lax.psum_scatter(
        jnp.dot(attended, whole_out, preferred_element_type=jnp.float32).astype(jnp.bfloat16),
        "tp",
        scatter_dimension=0,
        tiled=True,
    ).astype(jnp.float32)
    normed = mixed * lax.rsqrt(jnp.mean(mixed * mixed, axis=-1, keepdims=True) + 1e-06) * out_gain
    return normed.astype(jnp.bfloat16)


def solution(mesh):
    placed = (
        P(("dp", "kv"), None),
        P(("dp", "kv"), None),
        P("kv", "tp"),
        P("kv", "tp"),
        P("kv", "tp"),
        P("tp", "kv"),
        P(),
    )
    return jax.shard_map(
        per_device,
        mesh=mesh,
        in_specs=placed,
        out_specs=P(("dp", "kv", "tp"), None),
        check_vma=False,
    )
```

profile of v0, /device:TPU:17, one launch (start us, length us, event | category | flops | bytes accessed | tf_op | source)
XLA Modules:
  0.0 153.1 jit_solution(18030068477290165004)
XLA Ops:
  9.5 10.9 %all_gather.16 = bf16[2048,64]{0,1:T(8,128)(2,1)S(1)} all-gather(bf16[512,64]{0,1:T(8,128)(2,1)} %param.13), channel_id=1, replica_groups=mesh['dp'=4,'kv'=4,'tp'=2] {'kv'}, dimensions={0}, use_global_device_ids=true | all-gather | bytes 327680 | tf_op jit(solution)/shard_map/all_gather | solution.py:18
  20.5 14.8 %all_gather.15 = bf16[2048,64]{0,1:T(8,128)(2,1)S(1)} all-gather(bf16[512,64]{0,1:T(8,128)(2,1)} %param.12), channel_id=1, replica_groups=mesh['dp'=4,'kv'=4,'tp'=2] {'kv'}, dimensions={0}, use_global_device_ids=true | all-gather | bytes 327680 | tf_op jit(solution)/shard_map/all_gather | solution.py:17
  36.8 21.0 %all_gather.17 = bf16[2048,128]{0,1:T(8,128)(2,1)S(1)} all-gather(bf16[512,128]{0,1:T(8,128)(2,1)S(1)} %pad_maximum_fusion), channel_id=1, replica_groups=mesh['dp'=4,'kv'=4,'tp'=2] {'kv'}, dimensions={0}, use_global_device_ids=true | all-gather | bytes 655360 | tf_op jit(solution)/shard_map/all_gather | solution.py:30
  58.3 2.2 %gather_fusion = bf16[128,64,128]{2,1,0:T(8,128)(2,1)} fusion(bf16[32,64,128]{2,1,0:T(8,128)(2,1)S(1)} %bitcast.82, s32[1024]{0:T(1024)S(1)} %pad_clamp_fusion), kind=kCustom, calls=%fused_computation | custom fusion | bytes 4194816 | tf_op jit(solution)/shard_map/jit(_take)/gather | solution.py:33
  60.4 3.2 %broadcast_select_fusion = bf16[8,16,64,128]{3,2,1,0:T(8,128)(2,1)} fusion(bf16[8,16,64,128]{3,2,1,0:T(8,128)(2,1)} %bitcast.83, pred[8,16]{1,0:T(8,128)(4,1)S(1)} %get-tuple-element.56), kind=kLoop, calls=%fused_computation.27 | loop fusion | flops 1048576 | bytes 4194432 | tf_op jit(solution)/shard_map/jit(_take)/select_n | solution.py:33
  63.6 1.5 %compare_and_fusion = pred[8,64,16,64]{1,3,2,0:T(8,128)(4,1)S(1)} fusion(s32[8,64]{1,0:T(8,128)S(1)} %iota_add_fusion.1, s32[8,16,64]{2,1,0:T(8,128)S(1)} %iota_add_fusion, pred[8,16]{1,0:T(8,128)(4,1)S(1)} %get-tuple-element.55), kind=kLoop, calls=%fused_computation.20 | loop fusion | flops 1048576 | bytes 559232 | tf_op jit(solution)/shard_map/and | solution.py:41
  65.1 2.5 %all-gather.3.cloned.1.call-done = bf16[2048,512]{1,0:T(8,128)(2,1)} async-done(((bf16[512,512]{1,0:T(8,128)(2,1)}), bf16[2048,512]{1,0:T(8,128)(2,1)}) %all-gather.3.cloned.1.call-update) | async-done | bytes 2097168 | tf_op jit(solution)/shard_map/all_gather | solution.py:16
  67.6 3.6 %convolution_convert_fusion.1 = bf16[512,512]{1,0:T(8,128)(2,1)} fusion(bf16[512,2048]{1,0:T(8,128)(2,1)S(1)} %copy-done, bf16[2048,512]{1,0:T(8,128)(2,1)} %all-gather.3.cloned.1.call-done), kind=kOutput, calls=%fused_computation.28 | convolution fusion | flops 1074003968 | bytes 4718592 | tf_op jit(solution)/shard_map/dot_general | solution.py:20
  71.2 2.4 %reshape.58 = bf16[8,64,8,64]{3,2,1,0:T(8,128)(2,1)} reshape(bf16[512,512]{1,0:T(8,128)(2,1)} %convolution_convert_fusion.1) | data formatting | bytes 1048576 | tf_op jit(solution)/shard_map/reshape | solution.py:35
  73.6 47.3 %while.10 = (s32[]{:T(128)}, bf16[8,64,8,64]{3,2,1,0:T(8,128)(2,1)}, bf16[8,16,64,128]{3,2,1,0:T(8,128)(2,1)}, pred[8,64,16,64]{1,3,2,0:T(8,128)(4,1)S(1)}, bf16[8,64,8,64]{3,2,1,0:T(8,128)(2,1)}, /*index=5*/s32[]{:T(128)}) while((s32[]{:T(128)}, bf16[8,64,8,64]{3,2,1,0:T(8,128)(2,1)}, bf16[8,16,64,128]{3,2,1,0:T(8,128)(2,1)}, ...), condition=%wide.region_3.4_spmd, body=%wide.region_0.3_spmd.sunk | while | flops 140540928 | bytes 8268369 | solution.py:62
  77.5 1.2 fusion.25
  82.3 1.0 fusion.24
  83.4 1.2 fusion.25
  89.3 1.2 fusion.25
  95.2 1.2 fusion.25
  101.1 1.2 fusion.25
  107.0 1.2 fusion.25
  112.9 1.2 fusion.25
  118.8 1.2 fusion.25
  120.9 1.9 %reshape.59 = bf16[512,512]{1,0:T(8,128)(2,1)S(1)} reshape(bf16[8,64,8,64]{3,2,1,0:T(8,128)(2,1)} %get-tuple-element.32) | data formatting | bytes 1048576 | tf_op jit(solution)/shard_map/reshape | solution.py:63
  122.8 4.2 %convolution_convert_fusion = bf16[512,2048]{1,0:T(8,128)(2,1)} fusion(bf16[512,512]{1,0:T(8,128)(2,1)S(1)} %reshape.59, bf16[512,2048]{1,0:T(8,128)(2,1)} %all-gather.5.cloned.1.call-done), kind=kOutput, calls=%fused_computation.21 | convolution fusion | flops 1074790400 | bytes 4718592 | tf_op jit(solution)/shard_map/dot_general | solution.py:66
  127.0 15.5 %reduce-scatter.2.cloned.1.call-done = bf16[256,2048]{1,0:T(8,128)(2,1)} async-done(((bf16[512,2048]{1,0:T(8,128)(2,1)}), bf16[256,2048]{1,0:T(8,128)(2,1)}) %reduce-scatter.2.cloned.1.call-update) | async-done | bytes 1048592 | tf_op jit(solution)/shard_map/reduce_scatter | solution.py:65
  142.5 1.5 fusion.9
  144.0 2.5 %fusion.11 = bf16[256,2048]{1,0:T(8,128)(2,1)} fusion(bf16[256,2048]{1,0:T(8,128)(2,1)} %reduce-scatter.2.cloned.1.call-done, f32[2048]{0:T(1024)S(1)} %copy-done.1, f32[256]{0:T(256)S(1)} %add_rsqrt_fusion), kind=kLoop, calls=%fused_computation.26 | loop fusion | flops 2097152 | bytes 2106368 | tf_op jit(solution)/shard_map/convert_element_type | solution.py:72
  (79 shorter events, 41.0 us)
Async XLA Ops:
  6.5 28.7 %copy-start = (bf16[512,2048]{1,0:T(8,128)(2,1)S(1)}, bf16[512,2048]{1,0:T(8,128)(2,1)}, u32[]{:S(2)}) copy-start(bf16[512,2048]{1,0:T(8,128)(2,1)} %param.9) | copy-start | bytes 6291460
  6.5 61.1 %all-gather.3.cloned.1.call-start = ((), (), s32[]{:S(2)}) async-start(), calls=%async_computation.1 | async-start | bytes 2621440 | tf_op jit(solution)/shard_map/all_gather | solution.py:16
  7.3 115.5 %all-gather.5.cloned.1.call-start = ((), (), s32[]{:S(2)}) async-start(), calls=%async_computation.2 | async-start | bytes 2621440 | tf_op jit(solution)/shard_map/all_gather | solution.py:64
  8.0 134.5 %reduce-scatter.2.cloned.1.call-start = ((), (), s32[]{:S(2)}) async-start(), calls=%async_computation.3 | async-start | bytes 3145728 | tf_op jit(solution)/shard_map/reduce_scatter | solution.py:65
  127.0 17.1 %copy-start.1 = (f32[2048]{0:T(1024)S(1)}, f32[2048]{0:T(1024)}, u32[]{:S(2)}) copy-start(f32[2048]{0:T(1024)} %param.15) | copy-start | bytes 24580
Sparse Core Ops, SparseCore 0:
  8.9 58.6 all-gather.2
  69.2 44.7 all-gather.4
  127.1 15.3 reduce-scatter.1
where the time goes:
time: 155 us; the launch traced here: 153 us
  blocking collectives  46.7 us (30%)
  local copies, waits for them, and re-layouts  28.5 us (18%)
  matrix products  26.5 us (17%)
  waiting for transfers between devices  19.4 us (13%)
  other arithmetic  18.5 us (12%)
  between operations  13.2 us (9%)
    all_gather x1, blocking collectives, per_device(): lax.all_gather(paired, 'kv', axis=0, tiled=True)  21 us
    reduce_scatter x1, waiting for transfers between devices, per_device(): lax.psum_scatter(jnp.dot(attended, whole_out, preferred_element_type=jnp....  15.5 us
    all_gather x1, blocking collectives, per_device(): lax.all_gather(key_matrix, 'kv', axis=0, tiled=True)  14.8 us
    all_gather x1, blocking collectives, per_device(): lax.all_gather(value_matrix, 'kv', axis=0, tiled=True)  10.9 us
    dot_general x8, matrix products, attend_block(): jnp.einsum('gqsk,skd->qgd', weights_bf, block_values, preferred_element_t...  9.99 us
    reduce_sum x8, other arithmetic, attend_block(): row_sum = jnp.sum(expon, axis=(2, 3), keepdims=True)  8.16 us
    squeeze x8, local copies, waits for them, and re-layouts, per_device(): attended = lax.map(attend_block, (grouped, picked, visible))  7.8 us
    dynamic_slice x8, local copies, waits for them, and re-layouts, per_device(): attended = lax.map(attend_block, (grouped, picked, visible))  7.37 us
  transfers between devices with their start and end apart: 3, of which 2 were waited for; matrix products, arithmetic and copies ran while one was open for 43% of the time, Pallas kernels for 0%

commit v1 on v0

--- a/solution.py
+++ b/solution.py
@@ -1,10 +1,282 @@
+import functools
+
 import jax
 import jax.numpy as jnp
 from jax import lax
+from jax.experimental import pallas as pl
+from jax.experimental.pallas import tpu as pltpu
 from jax.sharding import PartitionSpec as P
 
 HEAD_WIDTH = 64
 BLOCK_LENGTH = 64
+LANES = 2 * HEAD_WIDTH
+HIDDEN = -1e30
+
+
+def remote(src, dst, send, recv, axis, peer):
+    return pltpu.make_async_remote_copy(
+        src_ref=src,
+        dst_ref=dst,
+        send_sem=send,
+        recv_sem=recv,
+        device_id={axis: peer},
+        device_id_type=pl.DeviceIdType.MESH,
+    )
+
+
+def fused(
+    n_dp, n_kv, n_tp,
+    chosen, tokens_hbm, pair_own, query_own, out_own, gain, result,
+    tokens, pair_all, query_all, out_all, kv_all, vk_all, query_sum, query_rows, attended,
+    leaving, arriving, kept,
+    token_sem, z_send, z_recv, d_send, d_recv, kv_send, kv_recv, t_send, t_recv,
+):
+    d, z, t = lax.axis_index("dp"), lax.axis_index("kv"), lax.axis_index("tp")
+    rows, width = tokens.shape
+    blocks = rows // BLOCK_LENGTH
+    depth = width // n_kv
+    half = rows // n_tp
+    token_copy = pltpu.make_async_copy(tokens_hbm, tokens, token_sem)
+    token_copy.start()
+
+    barrier = pltpu.get_barrier_semaphore()
+    for axis, me, count in (("dp", d, n_dp), ("kv", z, n_kv), ("tp", t, n_tp)):
+        for step in range(1, count):
+            pl.semaphore_signal(
+                barrier, inc=1, device_id={axis: lax.rem(me + step, count)},
+                device_id_type=pl.DeviceIdType.MESH,
+            )
+    pl.semaphore_wait(barrier, n_dp + n_kv + n_tp - 3)
+
+    owns = (pair_own, query_own, out_own)
+    alls = (pair_all, query_all, out_all)
+
+    def first(which, j):
+        return remote(
+            owns[which].at[d], alls[which].at[z, d], z_send.at[which, j], z_recv.at[which, j],
+            "kv", lax.rem(z + j, n_kv),
+        )
+
+    def first_in(which, j):
+        slot = alls[which].at[lax.rem(z + n_kv - j, n_kv), d]
+        return remote(
+            slot, slot, z_send.at[which, j], z_recv.at[which, j], "kv", lax.rem(z + j, n_kv)
+        )
+
+    def second(which, j, i):
+        slot = alls[which].at[lax.rem(z + n_kv - j, n_kv), d]
+        return remote(
+            slot, slot, d_send.at[which, j, i], d_recv.at[which, j, i],
+            "dp", lax.rem(d + i, n_dp),
+        )
+
+    def second_in(which, j, i):
+        slot = alls[which].at[lax.rem(z + n_kv - j, n_kv), lax.rem(d + n_dp - i, n_dp)]
+        return remote(
+            slot, slot, d_send.at[which, j, i], d_recv.at[which, j, i],
+            "dp", lax.rem(d + i, n_dp),
+        )
+
+    def pass_on(which):
+        for j in range(1, n_kv):
+            first_in(which, j).wait_recv()
+            for i in range(1, n_dp):
+                second(which, j, i).start()
+
+    def take(which, j):
+        if j:
+            for i in range(1, n_dp):
+                second_in(which, j, i).wait_recv()
+
+    def whole(which, j):
+        block = owns[which][...] if j == 0 else alls[which][lax.rem(z + n_kv - j, n_kv)]
+        return block.reshape(block.shape[0] * block.shape[1], block.shape[2])
+
+    def token_part(j):
+        start = pl.multiple_of(lax.rem(z + n_kv - j, n_kv) * depth, depth)
+        return tokens[:, pl.ds(start, depth)]
+
+    for which in (0, 1):
+        for j in range(1, n_kv):
+            first(which, j).start()
+    pass_on(0)
+    token_copy.wait()
+
+    total = jnp.dot(token_part(0), whole(0, 0), preferred_element_type=jnp.float32)
+    for j in range(1, n_kv):
+        take(0, j)
+        total += jnp.dot(token_part(j), whole(0, j), preferred_element_type=jnp.float32)
+    mine = kv_all.at[pl.ds(z * blocks, blocks)]
+    mine[...] = total.astype(jnp.bfloat16).reshape(blocks, BLOCK_LENGTH, LANES)
+
+    def kv_out(j):
+        return remote(mine, mine, kv_send.at[j], kv_recv.at[j], "kv", lax.rem(z + j, n_kv))
+
+    def kv_in(j):
+        slot = kv_all.at[pl.ds(lax.rem(z + n_kv - j, n_kv) * blocks, blocks)]
+        return remote(slot, slot, kv_send.at[j], kv_recv.at[j], "kv", lax.rem(z + j, n_kv))
+
+    for j in range(1, n_kv):
+        kv_out(j).start()
+    for j in range(1, n_kv):
+        first(2, j).start()
+    pass_on(1)
+
+    query_sum[...] = jnp.dot(token_part(0), whole(1, 0), preferred_element_type=jnp.float32)
+    for j in range(1, n_kv):
+        take(1, j)
+        query_sum[...] += jnp.dot(token_part(j), whole(1, j), preferred_element_type=jnp.float32)
+    query_rows[...] = query_sum[...].astype(jnp.bfloat16) * jnp.bfloat16(HEAD_WIDTH ** (-0.5))
+
+    pass_on(2)
+    for j in range(1, n_kv):
+        kv_in(j).wait_recv()
+
+    swap = (
+        lax.rem(lax.broadcasted_iota(jnp.int32, (LANES, LANES), 0) + HEAD_WIDTH, LANES)
+        == lax.broadcasted_iota(jnp.int32, (LANES, LANES), 1)
+    ).astype(jnp.float32).astype(jnp.bfloat16)
+    for j in range(n_kv):
+        part = kv_all[pl.ds(j * blocks, blocks)].reshape(rows, LANES)
+        turned = jnp.dot(part, swap, preferred_element_type=jnp.float32)
+        vk_all[pl.ds(j * blocks, blocks)] = turned.astype(jnp.bfloat16).reshape(
+            blocks, BLOCK_LENGTH, LANES
+        )
+
+    picks = chosen.shape[1]
+    pairs = query_rows.shape[1] // LANES
+
+    def attend(b, carry):
+        lane = lax.broadcasted_iota(jnp.int32, (BLOCK_LENGTH, LANES), 1)
+        row = lax.broadcasted_iota(jnp.int32, (BLOCK_LENGTH, LANES), 0)
+        low = (lane < HEAD_WIDTH).astype(jnp.float32)
+        names = [chosen[b, s] for s in range(picks)]
+        offs = [jnp.where(name >= 0, 0.0, HIDDEN) for name in names]
+        bias = []
+        for s in range(0, picks, 2):
+            tile = jnp.where(lane < HEAD_WIDTH, offs[s], offs[s + 1])
+            if s == 0:
+                tile = jnp.where((lane < HEAD_WIDTH) & (lane > row), HIDDEN, tile)
+            bias.append(tile)
+        bias = jnp.concatenate(bias, axis=1)
+        safe = [jnp.maximum(name, 0) for name in names]
+        kv = jnp.concatenate([kv_all[g] for g in safe], axis=0)
+        vk = jnp.concatenate([vk_all[g] for g in safe], axis=0)
+        at = pl.ds(pl.multiple_of(b * BLOCK_LENGTH, BLOCK_LENGTH), BLOCK_LENGTH)
+        query = query_rows[at, :]
+        stacked = jnp.concatenate(
+            [query[:, p * LANES : (p + 1) * LANES] for p in range(pairs)], axis=0
+        )
+        keep = jnp.concatenate([low] * pairs, axis=0)
+        outs = []
+        for side in range(2):
+            mask = keep if side == 0 else 1.0 - keep
+            masked = stacked * mask.astype(jnp.bfloat16)
+            keys, values = (kv, vk) if side == 0 else (vk, kv)
+            scores = lax.dot_general(
+                masked, keys, (((1,), (1,)), ((), ())), preferred_element_type=jnp.float32
+            )
+            scores = scores.reshape(pairs, BLOCK_LENGTH, picks * BLOCK_LENGTH) + bias[None]
+            top = jnp.max(scores, axis=2, keepdims=True)
+            expon = jnp.exp(scores - top)
+            inverse = 1.0 / jnp.sum(expon, axis=2, keepdims=True)
+            probs = (expon * inverse).astype(jnp.bfloat16)
+            probs = probs.reshape(pairs * BLOCK_LENGTH, picks * BLOCK_LENGTH)
+            outs.append(jnp.dot(probs, values, preferred_element_type=jnp.float32))
+        joined = jnp.where(keep > 0.5, outs[0], outs[1]).astype(jnp.bfloat16)
+        for p in range(pairs):
+            attended[at, p * LANES : (p + 1) * LANES] = joined[
+                p * BLOCK_LENGTH : (p + 1) * BLOCK_LENGTH
+            ]
+        return carry
+
+    lax.fori_loop(0, blocks, attend, 0)
+
+    peer = lax.rem(t + 1, n_tp)
+    other_rows = attended[pl.ds(pl.multiple_of(peer * half, half), half), :]
+    own_rows = attended[pl.ds(pl.multiple_of(t * half, half), half), :]
+
+    def swap_half(j):
+        slot = lax.rem(z + n_kv - j, n_kv)
+        return remote(
+            leaving.at[slot], arriving.at[slot], t_send.at[j], t_recv.at[j], "tp", peer
+        )
+
+    for j in range(n_kv):
+        take(2, j)
+        weight = whole(2, j)
+        slot = lax.rem(z + n_kv - j, n_kv)
+        leaving[slot] = jnp.dot(
+            other_rows, weight, preferred_element_type=jnp.float32
+        ).astype(jnp.bfloat16)
+        swap_half(j).start()
+        kept[slot] = jnp.dot(own_rows, weight, preferred_element_type=jnp.float32)
+
+    square = jnp.zeros((half, 1), jnp.float32)
+    for j in range(n_kv):
+        slot = lax.rem(z + n_kv - j, n_kv)
+        swap_half(j).wait_recv()
+        mixed = kept[slot] + arriving[slot].astype(jnp.float32)
+        kept[slot] = mixed
+        square += jnp.sum(mixed * mixed, axis=1, keepdims=True)
+    scale = lax.rsqrt(square * (1.0 / width) + 1e-06)
+    for j in range(n_kv):
+        columns = slice(j * depth, (j + 1) * depth)
+        result[:, columns] = (kept[j] * scale * gain[:, columns]).astype(jnp.bfloat16)
+
+    for which in range(3):
+        for j in range(1, n_kv):
+            first(which, j).wait_send()
+            for i in range(1, n_dp):
+                second(which, j, i).wait_send()
+    for j in range(1, n_kv):
+        kv_out(j).wait_send()
+    for j in range(n_kv):
+        swap_half(j).wait_send()
+
+
+def per_device_fused(
+    n_dp, n_kv, n_tp,
+    tokens, chosen, query_weight, key_matrix, value_matrix, out_weight, out_gain,
+):
+    rows, width = tokens.shape
+    depth, columns = query_weight.shape
+    blocks = rows // BLOCK_LENGTH
+    pair = jnp.concatenate([key_matrix, value_matrix], axis=1)
+    cut = lambda w: w.reshape(n_dp, w.shape[0] // n_dp, w.shape[1])
+    pair, query, out = cut(pair), cut(query_weight), cut(out_weight)
+    bf16, f32 = jnp.bfloat16, jnp.float32
+    vmem = pl.BlockSpec(memory_space=pltpu.VMEM)
+    dma = pltpu.SemaphoreType.DMA
+    return pl.pallas_call(
+        functools.partial(fused, n_dp, n_kv, n_tp),
+        out_shape=jax.ShapeDtypeStruct((rows // n_tp, width), bf16),
+        in_specs=[
+            pl.BlockSpec(memory_space=pltpu.SMEM),
+            pl.BlockSpec(memory_space=pl.ANY),
+            vmem, vmem, vmem, vmem,
+        ],
+        out_specs=vmem,
+        scratch_shapes=[
+            pltpu.VMEM((rows, width), bf16),
+            pltpu.VMEM((n_kv,) + pair.shape, bf16),
+            pltpu.VMEM((n_kv,) + query.shape, bf16),
+            pltpu.VMEM((n_kv,) + out.shape, bf16),
+            pltpu.VMEM((n_kv * blocks, BLOCK_LENGTH, LANES), bf16),
+            pltpu.VMEM((n_kv * blocks, BLOCK_LENGTH, LANES), bf16),
+            pltpu.VMEM((rows, columns), f32),
+            pltpu.VMEM((rows, columns), bf16),
+            pltpu.VMEM((rows, columns), bf16),
+            pltpu.VMEM((n_kv, rows // n_tp, width // n_kv), bf16),
+            pltpu.VMEM((n_kv, rows // n_tp, width // n_kv), bf16),
+            pltpu.VMEM((n_kv, rows // n_tp, width // n_kv), f32),
+            dma, dma((3, n_kv)), dma((3, n_kv)), dma((3, n_kv, n_dp)), dma((3, n_kv, n_dp)),
+            dma((n_kv,)), dma((n_kv,)), dma((n_kv,)), dma((n_kv,)),
+        ],
+        compiler_params=pltpu.CompilerParams(
+            collective_id=0, has_side_effects=True, vmem_limit_bytes=60 * 1024 * 1024
+        ),
+    )(chosen, tokens, pair, query, out, out_gain.reshape(1, width))
 
 
 def per_device(tokens, chosen, query_weight, key_matrix, value_matrix, out_weight, out_gain):
@@ -82,8 +354,27 @@
         P("tp", "kv"),
         P(),
     )
+    n_dp, n_kv, n_tp = (mesh.shape[name] for name in ("dp", "kv", "tp"))
+
+    def body(tokens, chosen, query_weight, key_matrix, value_matrix, out_weight, out_gain):
+        args = (tokens, chosen, query_weight, key_matrix, value_matrix, out_weight, out_gain)
+        depth, columns = query_weight.shape
+        whole_tiles = (
+            depth % (16 * n_dp) == 0
+            and out_weight.shape[0] % (16 * n_dp) == 0
+            and out_weight.shape[1] % LANES == 0
+            and depth % LANES == 0
+            and columns % LANES == 0
+            and key_matrix.shape[1] == HEAD_WIDTH
+            and chosen.shape[1] % 2 == 0
+            and n_tp == 2
+        )
+        if whole_tiles:
+            return per_device_fused(n_dp, n_kv, n_tp, *args)
+        return per_device(*args)
+
     return jax.shard_map(
-        per_device,
+        body,
         mesh=mesh,
         in_specs=placed,
         out_specs=P(("dp", "kv", "tp"), None),

time: 155 us -> 65.6 us (0.42); the launches traced: 153 us -> 65.4 us
  Pallas kernels: 0 us -> 61.4 us
  blocking collectives: 46.7 us -> 0 us
  matrix products: 26.5 us -> 0 us
  local copies, waits for them, and re-layouts: 28.5 us -> 3.07 us
  waiting for transfers between devices: 19.4 us -> 0 us
  other arithmetic: 18.5 us -> 0.88 us
  between operations: 13.2 us -> 0.01 us
    pallas_call x0 -> x1, Pallas kernels: none -> 61.4 us  [per_device_fused(): pl.pallas_call(functools.partial(fused, n_dp, n_kv, n_tp), out_shape=jax....]
    all_gather x3 -> x0, blocking collectives: 46.7 us -> none  [the longest x1 21 us: per_device(): lax.all_gather(paired, 'kv', axis=0, tiled=True)]
    dot_general x20 -> x0, matrix products: 26.5 us -> none  [the longest x8 9.99 us: attend_block(): jnp.einsum('gqsk,skd->qgd', weights_bf, block_values, preferred_element_t...]
    reduce_scatter x1 -> x0, waiting for transfers between devices: 15.5 us -> none  [per_device(): lax.psum_scatter(jnp.dot(attended, whole_out, preferred_element_type=jnp....]
    reduce_sum x9 -> x0, other arithmetic: 9.67 us -> none  [the longest x8 8.16 us: attend_block(): row_sum = jnp.sum(expon, axis=(2, 3), keepdims=True)]
    squeeze x8 -> x0, local copies, waits for them, and re-layouts: 7.8 us -> none  [per_device(): attended = lax.map(attend_block, (grouped, picked, visible))]
    dynamic_slice x8 -> x0, local copies, waits for them, and re-layouts: 7.37 us -> none  [per_device(): attended = lax.map(attend_block, (grouped, picked, visible))]
    dynamic_update_slice x16 -> x0, local copies, waits for them, and re-layouts: 6.49 us -> none  [per_device(): attended = lax.map(attend_block, (grouped, picked, visible))]
  transfers between devices with their start and end apart: 3 -> 0, of which waited for: 2 -> 0; matrix products, arithmetic and copies ran while one was open for 43% -> 0% of each run, Pallas kernels for 0% -> 0%
where the time goes in v1:
time: 65.6 us; the launch traced here: 65.4 us
  Pallas kernels  61.4 us (94%)
  local copies, waits for them, and re-layouts  3.07 us (5%)
  other arithmetic  0.88 us (1%)
    pallas_call x1, Pallas kernels, per_device_fused(): pl.pallas_call(functools.partial(fused, n_dp, n_kv, n_tp), out_shape=jax....  61.4 us
    unnamed x1, local copies, waits for them, and re-layouts  2.3 us

profile of v1, /device:TPU:17, one launch (start us, length us, event | category | flops | bytes accessed | tf_op | source)
XLA Modules:
  0.0 65.4 jit_solution(2329053715268698346)
XLA Ops:
  0.0 0.9 %pad_maximum_fusion = bf16[512,128]{0,1:T(8,128)(2,1)S(1)} fusion(bf16[512,64]{0,1:T(8,128)(2,1)} %param.11, bf16[512,64]{0,1:T(8,128)(2,1)} %param.10), kind=kLoop, calls=%fused_computation | loop fusion | flops 262144 | bytes 262144 | tf_op jit(solution)/shard_map/concatenate | solution.py:245
  0.9 0.8 %copy.8 = bf16[512,128]{1,0:T(8,128)(2,1)} copy(bf16[512,128]{0,1:T(8,128)(2,1)S(1)} %pad_maximum_fusion) | data formatting | bytes 262144 | tf_op jit(solution)/shard_map/concatenate | solution.py:245
  1.6 61.4 %shard_map.73 = bf16[256,2048]{1,0:T(8,128)(2,1)} custom-call(s32[8,16]{1,0:T(8,128)} %chosen.1, bf16[512,2048]{1,0:T(8,128)(2,1)} %tokens_hbm.1, bf16[4,128,128]{2,1,0:T(8,128)(2,1)} %bitcast.6, bf16[4,128,512]{2,1,0:T(8,128)(2,1)} %bitcast.4, bf16[4,128,512]{2,1,0:T(8,128)(2,1)} %bitcast.5, f32[1,2048]{1,0:T(1,128)} %bitcast.7), custom_call_target="tpu_custom_call" | custom-call | tf_op jit(solution)/shard_map/pallas_call | solution.py:251
  63.1 2.3 %copy.10 = bf16[256,2048]{1,0:T(8,128)(2,1)} copy(bf16[256,2048]{1,0:T(8,128)(2,1)} %shard_map.73) | data formatting | bytes 2097152

commit v2 on v1

--- a/solution.py
+++ b/solution.py
@@ -26,18 +26,35 @@
 
 def fused(
     n_dp, n_kv, n_tp,
-    chosen, tokens_hbm, pair_own, query_own, out_own, gain, result,
-    tokens, pair_all, query_all, out_all, kv_all, vk_all, query_sum, query_rows, attended,
+    chosen_hbm, tokens_hbm, key_hbm, value_hbm, query_hbm, out_hbm, gain_hbm, result,
+    chosen, gain, tokens, pair_own, query_own, out_own, pair_all, query_all, out_all, kv_all, vk_all, query_sum, query_rows, attended,
     leaving, arriving, kept,
-    token_sem, z_send, z_recv, d_send, d_recv, kv_send, kv_recv, t_send, t_recv,
+    load_sem, z_send, z_recv, d_send, d_recv, kv_send, kv_recv, t_send, t_recv,
 ):
     d, z, t = lax.axis_index("dp"), lax.axis_index("kv"), lax.axis_index("tp")
     rows, width = tokens.shape
     blocks = rows // BLOCK_LENGTH
     depth = width // n_kv
     half = rows // n_tp
-    token_copy = pltpu.make_async_copy(tokens_hbm, tokens, token_sem)
-    token_copy.start()
+    cut = depth // n_dp
+    loads = [
+        pltpu.make_async_copy(source, target, load_sem.at[k])
+        for k, (source, target) in enumerate(
+            ((query_hbm, query_own), (tokens_hbm, tokens), (out_hbm, out_own),
+             (gain_hbm, gain), (chosen_hbm, chosen))
+        )
+    ]
+    pair_loads = [
+        pltpu.make_async_copy(
+            source.at[:, k * cut : (k + 1) * cut],
+            pair_own.at[k, side * HEAD_WIDTH : (side + 1) * HEAD_WIDTH],
+            load_sem.at[5 + k * 2 + side],
+        )
+        for k in range(n_dp)
+        for side, source in enumerate((key_hbm, value_hbm))
+    ]
+    for load in pair_loads + loads:
+        load.start()
 
     barrier = pltpu.get_barrier_semaphore()
     for axis, me, count in (("dp", d, n_dp), ("kv", z, n_kv), ("tp", t, n_tp)):
@@ -77,11 +94,10 @@
             "dp", lax.rem(d + i, n_dp),
         )
 
-    def pass_on(which):
-        for j in range(1, n_kv):
-            first_in(which, j).wait_recv()
-            for i in range(1, n_dp):
-                second(which, j, i).start()
+    def pass_on(which, j):
+        first_in(which, j).wait_recv()
+        for i in range(1, n_dp):
+            second(which, j, i).start()
 
     def take(which, j):
         if j:
@@ -97,15 +113,28 @@
         return tokens[:, pl.ds(start, depth)]
 
     for which in (0, 1):
+        for load in (pair_loads, loads[:1])[which]:
+            load.wait()
         for j in range(1, n_kv):
             first(which, j).start()
-    pass_on(0)
-    token_copy.wait()
-
-    total = jnp.dot(token_part(0), whole(0, 0), preferred_element_type=jnp.float32)
+    for j in range(1, n_kv):
+        pass_on(0, j)
+    if n_kv > 1:
+        pass_on(1, 1)
+    for load in loads[1:]:
+        load.wait()
+
+    def pair_part(j):
+        block = pair_own[...] if j == 0 else pair_all[lax.rem(z + n_kv - j, n_kv)]
+        block = jnp.concatenate([block[k] for k in range(n_dp)], axis=1)
+        return lax.dot_general(
+            token_part(j), block, (((1,), (1,)), ((), ())), preferred_element_type=jnp.float32
+        )
+
+    total = pair_part(0)
     for j in range(1, n_kv):
         take(0, j)
-        total += jnp.dot(token_part(j), whole(0, j), preferred_element_type=jnp.float32)
+        total += pair_part(j)
     mine = kv_all.at[pl.ds(z * blocks, blocks)]
     mine[...] = total.astype(jnp.bfloat16).reshape(blocks, BLOCK_LENGTH, LANES)
 
@@ -120,7 +149,8 @@
         kv_out(j).start()
     for j in range(1, n_kv):
         first(2, j).start()
-    pass_on(1)
+    for j in range(2, n_kv):
+        pass_on(1, j)
 
     query_sum[...] = jnp.dot(token_part(0), whole(1, 0), preferred_element_type=jnp.float32)
     for j in range(1, n_kv):
@@ -128,7 +158,6 @@
         query_sum[...] += jnp.dot(token_part(j), whole(1, j), preferred_element_type=jnp.float32)
     query_rows[...] = query_sum[...].astype(jnp.bfloat16) * jnp.bfloat16(HEAD_WIDTH ** (-0.5))
 
-    pass_on(2)
     for j in range(1, n_kv):
         kv_in(j).wait_recv()
 
@@ -147,6 +176,12 @@
     pairs = query_rows.shape[1] // LANES
 
     def attend(b, carry):
+        for j in range(1, n_kv):
+
+            @pl.when(b == min(2 * j, blocks - 1))
+            def _(j=j):
+                pass_on(2, j)
+
         lane = lax.broadcasted_iota(jnp.int32, (BLOCK_LENGTH, LANES), 1)
         row = lax.broadcasted_iota(jnp.int32, (BLOCK_LENGTH, LANES), 0)
         low = (lane < HEAD_WIDTH).astype(jnp.float32)
@@ -180,9 +215,10 @@
             top = jnp.max(scores, axis=2, keepdims=True)
             expon = jnp.exp(scores - top)
             inverse = 1.0 / jnp.sum(expon, axis=2, keepdims=True)
-            probs = (expon * inverse).astype(jnp.bfloat16)
+            probs = expon.astype(jnp.bfloat16)
             probs = probs.reshape(pairs * BLOCK_LENGTH, picks * BLOCK_LENGTH)
-            outs.append(jnp.dot(probs, values, preferred_element_type=jnp.float32))
+            out = jnp.dot(probs, values, preferred_element_type=jnp.float32)
+            outs.append(out * inverse.reshape(pairs * BLOCK_LENGTH, 1))
         joined = jnp.where(keep > 0.5, outs[0], outs[1]).astype(jnp.bfloat16)
         for p in range(pairs):
             attended[at, p * LANES : (p + 1) * LANES] = joined[
@@ -242,23 +278,27 @@
     rows, width = tokens.shape
     depth, columns = query_weight.shape
     blocks = rows // BLOCK_LENGTH
-    pair = jnp.concatenate([key_matrix, value_matrix], axis=1)
     cut = lambda w: w.reshape(n_dp, w.shape[0] // n_dp, w.shape[1])
-    pair, query, out = cut(pair), cut(query_weight), cut(out_weight)
+    query, out = cut(query_weight), cut(out_weight)
+    pair = jax.ShapeDtypeStruct((n_dp, LANES, depth // n_dp), jnp.bfloat16)
     bf16, f32 = jnp.bfloat16, jnp.float32
     vmem = pl.BlockSpec(memory_space=pltpu.VMEM)
+    off_core = pl.BlockSpec(memory_space=pltpu.HBM)
     dma = pltpu.SemaphoreType.DMA
     return pl.pallas_call(
         functools.partial(fused, n_dp, n_kv, n_tp),
         out_shape=jax.ShapeDtypeStruct((rows // n_tp, width), bf16),
         in_specs=[
-            pl.BlockSpec(memory_space=pltpu.SMEM),
-            pl.BlockSpec(memory_space=pl.ANY),
-            vmem, vmem, vmem, vmem,
+            off_core, off_core, off_core, off_core, off_core, off_core, off_core,
         ],
         out_specs=vmem,
         scratch_shapes=[
+            pltpu.SMEM((blocks, chosen.shape[1]), jnp.int32),
+            pltpu.VMEM((1, width), f32),
             pltpu.VMEM((rows, width), bf16),
+            pltpu.VMEM(pair.shape, bf16),
+            pltpu.VMEM(query.shape, bf16),
+            pltpu.VMEM(out.shape, bf16),
             pltpu.VMEM((n_kv,) + pair.shape, bf16),
             pltpu.VMEM((n_kv,) + query.shape, bf16),
             pltpu.VMEM((n_kv,) + out.shape, bf16),
@@ -270,13 +310,13 @@
             pltpu.VMEM((n_kv, rows // n_tp, width // n_kv), bf16),
             pltpu.VMEM((n_kv, rows // n_tp, width // n_kv), bf16),
             pltpu.VMEM((n_kv, rows // n_tp, width // n_kv), f32),
-            dma, dma((3, n_kv)), dma((3, n_kv)), dma((3, n_kv, n_dp)), dma((3, n_kv, n_dp)),
+            dma((5 + 2 * n_dp,)), dma((3, n_kv)), dma((3, n_kv)), dma((3, n_kv, n_dp)), dma((3, n_kv, n_dp)),
             dma((n_kv,)), dma((n_kv,)), dma((n_kv,)), dma((n_kv,)),
         ],
         compiler_params=pltpu.CompilerParams(
-            collective_id=0, has_side_effects=True, vmem_limit_bytes=60 * 1024 * 1024
+            collective_id=0, has_side_effects=True, vmem_limit_bytes=54 * 1024 * 1024
         ),
-    )(chosen, tokens, pair, query, out, out_gain.reshape(1, width))
+    )(chosen, tokens, key_matrix.T, value_matrix.T, query, out, out_gain.reshape(1, width))
 
 
 def per_device(tokens, chosen, query_weight, key_matrix, value_matrix, out_weight, out_gain):
@@ -360,10 +400,9 @@
         args = (tokens, chosen, query_weight, key_matrix, value_matrix, out_weight, out_gain)
         depth, columns = query_weight.shape
         whole_tiles = (
-            depth % (16 * n_dp) == 0
+            depth % (LANES * n_dp) == 0
             and out_weight.shape[0] % (16 * n_dp) == 0
             and out_weight.shape[1] % LANES == 0
-            and depth % LANES == 0
             and columns % LANES == 0
             and key_matrix.shape[1] == HEAD_WIDTH
             and chosen.shape[1] % 2 == 0

time: 65.6 us -> 63.3 us (0.965)
  Pallas kernels: 61.4 us -> 60.3 us
  other arithmetic: 0.88 us -> 0 us
  local copies, waits for them, and re-layouts: 3.07 us -> 2.3 us
    pallas_call x1, Pallas kernels: 61.4 us -> 60.3 us  [per_device_fused(): pl.pallas_call(functools.partial(fused, n_dp, n_kv, n_tp), out_shape=jax....]
    concatenate x1 -> x0, other arithmetic: 0.88 us -> none  [per_device_fused(): pair = jnp.concatenate([key_matrix, value_matrix], axis=1)]
    concatenate x1 -> x0, local copies, waits for them, and re-layouts: 0.76 us -> none  [per_device_fused(): pair = jnp.concatenate([key_matrix, value_matrix], axis=1)]
where the time goes in v2:
time: 63.3 us; the launch traced here: 62.6 us
  Pallas kernels  60.3 us (95%)
  local copies, waits for them, and re-layouts  2.3 us (4%)
    pallas_call x1, Pallas kernels, per_device_fused(): pl.pallas_call(functools.partial(fused, n_dp, n_kv, n_tp), out_shape=jax....  60.3 us
    unnamed x1, local copies, waits for them, and re-layouts  2.3 us

profile of v2, /device:TPU:17, one launch (start us, length us, event | category | flops | bytes accessed | tf_op | source)
XLA Modules:
  0.0 62.6 jit_solution(2918595821972065159)
XLA Ops:
  0.0 60.3 %shard_map.73 = bf16[256,2048]{1,0:T(8,128)(2,1)} custom-call(s32[8,16]{1,0:T(8,128)} %chosen_hbm.1, bf16[512,2048]{1,0:T(8,128)(2,1)} %tokens_hbm.1, bf16[64,512]{1,0:T(8,128)(2,1)} %bitcast.7, bf16[64,512]{1,0:T(8,128)(2,1)} %bitcast.8, bf16[4,128,512]{2,1,0:T(8,128)(2,1)} %bitcast.5, bf16[4,128,512]{2,1,0:T(8,128)(2,1)} %bitcast.6, f32[1,2048]{1,0:T(1,128)} %bitcast.9), custom_call_target="tpu_custom_call" | custom-call | tf_op jit(solution)/shard_map/pallas_call | solution.py:288
  60.3 2.3 %copy.9 = bf16[256,2048]{1,0:T(8,128)(2,1)} copy(bf16[256,2048]{1,0:T(8,128)(2,1)} %shard_map.73) | data formatting | bytes 2097152

commit v3 on v2

--- a/solution.py
+++ b/solution.py
@@ -11,6 +11,7 @@
 BLOCK_LENGTH = 64
 LANES = 2 * HEAD_WIDTH
 HIDDEN = -1e30
+CAP = 2
 
 
 def remote(src, dst, send, recv, axis, peer):
@@ -27,9 +28,10 @@
 def fused(
     n_dp, n_kv, n_tp,
     chosen_hbm, tokens_hbm, key_hbm, value_hbm, query_hbm, out_hbm, gain_hbm, result,
-    chosen, gain, tokens, pair_own, query_own, out_own, pair_all, query_all, out_all, kv_all, vk_all, query_sum, query_rows, attended,
+    chosen, gain, tokens, pair_own, query_own, out_own, wanted, asks, packed, kv_own, kv_far,
+    pair_all, query_all, out_all, kv_all, vk_all, query_sum, query_rows, attended,
     leaving, arriving, kept,
-    load_sem, z_send, z_recv, d_send, d_recv, kv_send, kv_recv, t_send, t_recv,
+    load_sem, z_send, z_recv, d_send, d_recv, r_send, r_recv, kv_send, kv_recv, t_send, t_recv, ask_send, ask_recv,
 ):
     d, z, t = lax.axis_index("dp"), lax.axis_index("kv"), lax.axis_index("tp")
     rows, width = tokens.shape
@@ -41,14 +43,14 @@
         pltpu.make_async_copy(source, target, load_sem.at[k])
         for k, (source, target) in enumerate(
             ((query_hbm, query_own), (tokens_hbm, tokens), (out_hbm, out_own),
-             (gain_hbm, gain), (chosen_hbm, chosen))
+             (gain_hbm, gain), (chosen_hbm, wanted), (chosen_hbm, chosen))
         )
     ]
     pair_loads = [
         pltpu.make_async_copy(
             source.at[:, k * cut : (k + 1) * cut],
             pair_own.at[k, side * HEAD_WIDTH : (side + 1) * HEAD_WIDTH],
-            load_sem.at[5 + k * 2 + side],
+            load_sem.at[6 + k * 2 + side],
         )
         for k in range(n_dp)
         for side, source in enumerate((key_hbm, value_hbm))
@@ -80,29 +82,38 @@
             slot, slot, z_send.at[which, j], z_recv.at[which, j], "kv", lax.rem(z + j, n_kv)
         )
 
-    def second(which, j, i):
-        slot = alls[which].at[lax.rem(z + n_kv - j, n_kv), d]
-        return remote(
-            slot, slot, d_send.at[which, j, i], d_recv.at[which, j, i],
-            "dp", lax.rem(d + i, n_dp),
-        )
-
-    def second_in(which, j, i):
-        slot = alls[which].at[lax.rem(z + n_kv - j, n_kv), lax.rem(d + n_dp - i, n_dp)]
-        return remote(
-            slot, slot, d_send.at[which, j, i], d_recv.at[which, j, i],
-            "dp", lax.rem(d + i, n_dp),
-        )
+    near = (d, d + 1 - 2 * lax.rem(d, 2), lax.rem(d + 2, 4))
+    corner = 3 - d
+
+    def second(which, j, k, place=None):
+        slot = alls[which].at[lax.rem(z + n_kv - j, n_kv), d if place is None else place]
+        return remote(
+            slot, slot, d_send.at[which, j, k], d_recv.at[which, j, k], "dp", near[k]
+        )
+
+    def halfway(which, j, k, place):
+        rows_half = owns[which].shape[1] // 2
+        slot = alls[which].at[
+            lax.rem(z + n_kv - j, n_kv), place, (k - 1) * rows_half : k * rows_half
+        ]
+        return remote(
+            slot, slot, r_send.at[which, j, k], r_recv.at[which, j, k], "dp", near[3 - k]
+        )
+
+    def relay(which, j):
+        for k in (1, 2):
+            second(which, j, k, near[k]).wait_recv()
+            halfway(which, j, k, near[k]).start()
 
     def pass_on(which, j):
         first_in(which, j).wait_recv()
-        for i in range(1, n_dp):
-            second(which, j, i).start()
+        for k in (1, 2):
+            second(which, j, k).start()
 
     def take(which, j):
         if j:
-            for i in range(1, n_dp):
-                second_in(which, j, i).wait_recv()
+            for k in (1, 2):
+                halfway(which, j, k, corner).wait_recv()
 
     def whole(which, j):
         block = owns[which][...] if j == 0 else alls[which][lax.rem(z + n_kv - j, n_kv)]
@@ -112,6 +123,20 @@
         start = pl.multiple_of(lax.rem(z + n_kv - j, n_kv) * depth, depth)
         return tokens[:, pl.ds(start, depth)]
 
+    def ask(j):
+        return remote(
+            wanted, asks.at[z], ask_send.at[j], ask_recv.at[j], "kv", lax.rem(z + n_kv - j, n_kv)
+        )
+
+    def ask_in(j):
+        slot = asks.at[lax.rem(z + j, n_kv)]
+        return remote(
+            slot, slot, ask_send.at[j], ask_recv.at[j], "kv", lax.rem(z + n_kv - j, n_kv)
+        )
+
+    loads[4].wait()
+    for j in range(1, n_kv):
+        ask(j).start()
     for which in (0, 1):
         for load in (pair_loads, loads[:1])[which]:
             load.wait()
@@ -121,7 +146,7 @@
         pass_on(0, j)
     if n_kv > 1:
         pass_on(1, 1)
-    for load in loads[1:]:
+    for load in loads[1:4] + loads[5:]:
         load.wait()
 
     def pair_part(j):
@@ -133,27 +158,51 @@
 
     total = pair_part(0)
     for j in range(1, n_kv):
+        relay(0, j)
+    for j in range(1, n_kv):
         take(0, j)
         total += pair_part(j)
-    mine = kv_all.at[pl.ds(z * blocks, blocks)]
-    mine[...] = total.astype(jnp.bfloat16).reshape(blocks, BLOCK_LENGTH, LANES)
+    kv_own[...] = total.astype(jnp.bfloat16).reshape(blocks, BLOCK_LENGTH, LANES)
+
+    def named(rows_of, owner):
+        local = rows_of - owner * blocks
+        inside = (local >= 0) & (local < blocks)
+        return (
+            jnp.min(jnp.where(inside, local, blocks - 1)),
+            jnp.max(jnp.where(inside, local, 0)),
+        )
 
     def kv_out(j):
-        return remote(mine, mine, kv_send.at[j], kv_recv.at[j], "kv", lax.rem(z + j, n_kv))
+        return remote(
+            packed.at[j], kv_far.at[pl.ds(z * CAP, CAP)], kv_send.at[j], kv_recv.at[j],
+            "kv", lax.rem(z + j, n_kv),
+        )
 
     def kv_in(j):
-        slot = kv_all.at[pl.ds(lax.rem(z + n_kv - j, n_kv) * blocks, blocks)]
+        slot = kv_far.at[pl.ds(lax.rem(z + n_kv - j, n_kv) * CAP, CAP)]
         return remote(slot, slot, kv_send.at[j], kv_recv.at[j], "kv", lax.rem(z + j, n_kv))
 
+    kv_far[pl.ds(z * CAP, CAP)] = jnp.zeros((CAP, BLOCK_LENGTH, LANES), jnp.bfloat16)
+    for j in range(1, n_kv):
+        ask_in(j).wait_recv()
+        lowest, highest = named(asks[lax.rem(z + j, n_kv)], z)
+        packed[j, 0] = kv_own[lowest]
+        packed[j, 1] = kv_own[highest]
+    firsts = [named(wanted[...], owner)[0] + owner * blocks for owner in range(n_kv)]
     for j in range(1, n_kv):
         kv_out(j).start()
     for j in range(1, n_kv):
         first(2, j).start()
     for j in range(2, n_kv):
         pass_on(1, j)
+        relay(1, j - 1)
+    if n_kv > 1:
+        relay(1, n_kv - 1)
 
     query_sum[...] = jnp.dot(token_part(0), whole(1, 0), preferred_element_type=jnp.float32)
     for j in range(1, n_kv):
+        if j == n_kv - 1:
+            pass_on(2, 1)
         take(1, j)
         query_sum[...] += jnp.dot(token_part(j), whole(1, j), preferred_element_type=jnp.float32)
     query_rows[...] = query_sum[...].astype(jnp.bfloat16) * jnp.bfloat16(HEAD_WIDTH ** (-0.5))
@@ -165,12 +214,14 @@
         lax.rem(lax.broadcasted_iota(jnp.int32, (LANES, LANES), 0) + HEAD_WIDTH, LANES)
         == lax.broadcasted_iota(jnp.int32, (LANES, LANES), 1)
     ).astype(jnp.float32).astype(jnp.bfloat16)
-    for j in range(n_kv):
-        part = kv_all[pl.ds(j * blocks, blocks)].reshape(rows, LANES)
-        turned = jnp.dot(part, swap, preferred_element_type=jnp.float32)
-        vk_all[pl.ds(j * blocks, blocks)] = turned.astype(jnp.bfloat16).reshape(
-            blocks, BLOCK_LENGTH, LANES
-        )
+    for source, start in ((kv_far, 0), (kv_own, n_kv * CAP)):
+        count = source.shape[0]
+        part = source[...]
+        turned = jnp.dot(
+            part.reshape(count * BLOCK_LENGTH, LANES), swap, preferred_element_type=jnp.float32
+        )
+        kv_all[start : start + count] = part
+        vk_all[start : start + count] = turned.astype(jnp.bfloat16).reshape(part.shape)
 
     picks = chosen.shape[1]
     pairs = query_rows.shape[1] // LANES
@@ -178,9 +229,14 @@
     def attend(b, carry):
         for j in range(1, n_kv):
 
+            @pl.when(b == min(2 * (j - 1), blocks - 1))
+            def _(j=j):
+                if j < n_kv - 1:
+                    pass_on(2, j + 1)
+
             @pl.when(b == min(2 * j, blocks - 1))
             def _(j=j):
-                pass_on(2, j)
+                relay(2, j)
 
         lane = lax.broadcasted_iota(jnp.int32, (BLOCK_LENGTH, LANES), 1)
         row = lax.broadcasted_iota(jnp.int32, (BLOCK_LENGTH, LANES), 0)
@@ -194,7 +250,18 @@
                 tile = jnp.where((lane < HEAD_WIDTH) & (lane > row), HIDDEN, tile)
             bias.append(tile)
         bias = jnp.concatenate(bias, axis=1)
-        safe = [jnp.maximum(name, 0) for name in names]
+
+        def place(name):
+            name = jnp.maximum(name, 0)
+            spot = name - z * blocks + n_kv * CAP
+            for owner in range(n_kv):
+                local = name - owner * blocks
+                away = (local >= 0) & (local < blocks) & (z != owner)
+                far = owner * CAP + jnp.where(name == firsts[owner], 0, 1)
+                spot = jnp.where(away, far, spot)
+            return spot
+
+        safe = [jnp.where(name >= 0, place(name), 0) for name in names]
         kv = jnp.concatenate([kv_all[g] for g in safe], axis=0)
         vk = jnp.concatenate([vk_all[g] for g in safe], axis=0)
         at = pl.ds(pl.multiple_of(b * BLOCK_LENGTH, BLOCK_LENGTH), BLOCK_LENGTH)
@@ -263,10 +330,12 @@
     for which in range(3):
         for j in range(1, n_kv):
             first(which, j).wait_send()
-            for i in range(1, n_dp):
-                second(which, j, i).wait_send()
+            for k in (1, 2):
+                second(which, j, k).wait_send()
+                halfway(which, j, k, near[k]).wait_send()
     for j in range(1, n_kv):
         kv_out(j).wait_send()
+        ask(j).wait_send()
     for j in range(n_kv):
         swap_half(j).wait_send()
 
@@ -299,19 +368,26 @@
             pltpu.VMEM(pair.shape, bf16),
             pltpu.VMEM(query.shape, bf16),
             pltpu.VMEM(out.shape, bf16),
+            pltpu.VMEM((blocks, chosen.shape[1]), jnp.int32),
+            pltpu.VMEM((n_kv, blocks, chosen.shape[1]), jnp.int32),
+            pltpu.VMEM((n_kv, CAP, BLOCK_LENGTH, LANES), bf16),
+            pltpu.VMEM((blocks, BLOCK_LENGTH, LANES), bf16),
+            pltpu.VMEM((n_kv * CAP, BLOCK_LENGTH, LANES), bf16),
             pltpu.VMEM((n_kv,) + pair.shape, bf16),
             pltpu.VMEM((n_kv,) + query.shape, bf16),
             pltpu.VMEM((n_kv,) + out.shape, bf16),
-            pltpu.VMEM((n_kv * blocks, BLOCK_LENGTH, LANES), bf16),
-            pltpu.VMEM((n_kv * blocks, BLOCK_LENGTH, LANES), bf16),
+            pltpu.VMEM((n_kv * CAP + blocks, BLOCK_LENGTH, LANES), bf16),
+            pltpu.VMEM((n_kv * CAP + blocks, BLOCK_LENGTH, LANES), bf16),
             pltpu.VMEM((rows, columns), f32),
             pltpu.VMEM((rows, columns), bf16),
             pltpu.VMEM((rows, columns), bf16),
             pltpu.VMEM((n_kv, rows // n_tp, width // n_kv), bf16),
             pltpu.VMEM((n_kv, rows // n_tp, width // n_kv), bf16),
             pltpu.VMEM((n_kv, rows // n_tp, width // n_kv), f32),
-            dma((5 + 2 * n_dp,)), dma((3, n_kv)), dma((3, n_kv)), dma((3, n_kv, n_dp)), dma((3, n_kv, n_dp)),
+            dma((6 + 2 * n_dp,)), dma((3, n_kv)), dma((3, n_kv)), dma((3, n_kv, 3)), dma((3, n_kv, 3)),
+            dma((3, n_kv, 3)), dma((3, n_kv, 3)),
             dma((n_kv,)), dma((n_kv,)), dma((n_kv,)), dma((n_kv,)),
+            dma((n_kv,)), dma((n_kv,)),
         ],
         compiler_params=pltpu.CompilerParams(
             collective_id=0, has_side_effects=True, vmem_limit_bytes=54 * 1024 * 1024
@@ -407,6 +483,7 @@
             and key_matrix.shape[1] == HEAD_WIDTH
             and chosen.shape[1] % 2 == 0
             and n_tp == 2
+            and n_dp == 4
         )
         if whole_tiles:
             return per_device_fused(n_dp, n_kv, n_tp, *args)

time: 63.3 us -> 58.9 us (0.930)
  Pallas kernels: 60.3 us -> 56.4 us
    pallas_call x1, Pallas kernels: 60.3 us -> 56.4 us  [per_device_fused(): pl.pallas_call(functools.partial(fused, n_dp, n_kv, n_tp), out_shape=jax....]
where the time goes in v3:
time: 58.9 us; the launch traced here: 58.7 us
  Pallas kernels  56.4 us (96%)
  local copies, waits for them, and re-layouts  2.3 us (4%)
    pallas_call x1, Pallas kernels, per_device_fused(): pl.pallas_call(functools.partial(fused, n_dp, n_kv, n_tp), out_shape=jax....  56.4 us
    unnamed x1, local copies, waits for them, and re-layouts  2.3 us

profile of v3, /device:TPU:17, one launch (start us, length us, event | category | flops | bytes accessed | tf_op | source)
XLA Modules:
  0.0 58.7 jit_solution(13002054354739010244)
XLA Ops:
  0.0 56.4 %shard_map.73 = bf16[256,2048]{1,0:T(8,128)(2,1)} custom-call(s32[8,16]{1,0:T(8,128)} %chosen_hbm.1, bf16[512,2048]{1,0:T(8,128)(2,1)} %tokens_hbm.1, bf16[64,512]{1,0:T(8,128)(2,1)} %bitcast.7, bf16[64,512]{1,0:T(8,128)(2,1)} %bitcast.8, bf16[4,128,512]{2,1,0:T(8,128)(2,1)} %bitcast.5, bf16[4,128,512]{2,1,0:T(8,128)(2,1)} %bitcast.6, f32[1,2048]{1,0:T(1,128)} %bitcast.9), custom_call_target="tpu_custom_call" | custom-call | tf_op jit(solution)/shard_map/pallas_call | solution.py:357
  56.4 2.3 %copy.9 = bf16[256,2048]{1,0:T(8,128)(2,1)} copy(bf16[256,2048]{1,0:T(8,128)(2,1)} %shard_map.73) | data formatting | bytes 2097152

commit v4 on v3

--- a/solution.py
+++ b/solution.py
@@ -144,8 +144,13 @@
             first(which, j).start()
     for j in range(1, n_kv):
         pass_on(0, j)
-    if n_kv > 1:
-        pass_on(1, 1)
+    for j in range(1, n_kv):
+        pass_on(1, j)
+        if j == 1:
+            for k in range(1, n_kv):
+                relay(0, k)
+        elif j < n_kv - 1:
+            relay(1, j - 1)
     for load in loads[1:4] + loads[5:]:
         load.wait()
 
@@ -157,8 +162,6 @@
         )
 
     total = pair_part(0)
-    for j in range(1, n_kv):
-        relay(0, j)
     for j in range(1, n_kv):
         take(0, j)
         total += pair_part(j)
@@ -191,18 +194,13 @@
     firsts = [named(wanted[...], owner)[0] + owner * blocks for owner in range(n_kv)]
     for j in range(1, n_kv):
         kv_out(j).start()
+    for j in range(max(n_kv - 2, 1), n_kv):
+        relay(1, j)
     for j in range(1, n_kv):
         first(2, j).start()
-    for j in range(2, n_kv):
-        pass_on(1, j)
-        relay(1, j - 1)
-    if n_kv > 1:
-        relay(1, n_kv - 1)
 
     query_sum[...] = jnp.dot(token_part(0), whole(1, 0), preferred_element_type=jnp.float32)
     for j in range(1, n_kv):
-        if j == n_kv - 1:
-            pass_on(2, 1)
         take(1, j)
         query_sum[...] += jnp.dot(token_part(j), whole(1, j), preferred_element_type=jnp.float32)
     query_rows[...] = query_sum[...].astype(jnp.bfloat16) * jnp.bfloat16(HEAD_WIDTH ** (-0.5))
@@ -229,12 +227,11 @@
     def attend(b, carry):
         for j in range(1, n_kv):
 
-            @pl.when(b == min(2 * (j - 1), blocks - 1))
+            @pl.when(b == min(j, blocks - 1))
             def _(j=j):
-                if j < n_kv - 1:
-                    pass_on(2, j + 1)
-
-            @pl.when(b == min(2 * j, blocks - 1))
+                pass_on(2, j)
+
+            @pl.when(b == min(j + 4, blocks - 1))
             def _(j=j):
                 relay(2, j)
 

time: 58.9 us -> 55.5 us (0.942)
  the two profiles are of different devices: /device:TPU:17 before, /device:TPU:1 now
where the time goes in v4:
time: 55.5 us; the launch traced here: 55.4 us
  Pallas kernels  53.1 us (96%)
  local copies, waits for them, and re-layouts  2.3 us (4%)
    pallas_call x1, Pallas kernels, per_device_fused(): pl.pallas_call(functools.partial(fused, n_dp, n_kv, n_tp), out_shape=jax....  53.1 us
    unnamed x1, local copies, waits for them, and re-layouts  2.3 us

profile of v4, /device:TPU:1, one launch (start us, length us, event | category | flops | bytes accessed | tf_op | source)
XLA Modules:
  0.0 55.4 jit_solution(6420760823686496147)
XLA Ops:
  0.0 53.1 %shard_map.73 = bf16[256,2048]{1,0:T(8,128)(2,1)} custom-call(s32[8,16]{1,0:T(8,128)} %chosen_hbm.1, bf16[512,2048]{1,0:T(8,128)(2,1)} %tokens_hbm.1, bf16[64,512]{1,0:T(8,128)(2,1)} %bitcast.7, bf16[64,512]{1,0:T(8,128)(2,1)} %bitcast.8, bf16[4,128,512]{2,1,0:T(8,128)(2,1)} %bitcast.5, bf16[4,128,512]{2,1,0:T(8,128)(2,1)} %bitcast.6, f32[1,2048]{1,0:T(1,128)} %bitcast.9), custom_call_target="tpu_custom_call" | custom-call | tf_op jit(solution)/shard_map/pallas_call | solution.py:354
  53.1 2.3 %copy.9 = bf16[256,2048]{1,0:T(8,128)(2,1)} copy(bf16[256,2048]{1,0:T(8,128)(2,1)} %shard_map.73) | data formatting | bytes 2097152
